TPU v7x, 512 devices: a whole 4x4x16 slice. The times are simulated.
512 devices in a mesh: kv: 32 (over z, core), tp: 16 (over y, x).
Axes of the slice: x: 4, y: 4, z: 16, core: 2. Of those that a mesh axis runs over, the one named last changes fastest.
Arguments:
- tokens: bfloat16 [24, 4096], P(None, 'kv'), may hold values from -24 to 24
- attention_norm_gain: float32 [4096], replicated, may hold values from 0.1 to 1.9
- query_weight: bfloat16 [4096, 2048], P('kv', 'tp'), may hold values from -0.09375 to 0.09375
- key_weight: bfloat16 [4096, 2048], P('kv', 'tp'), may hold values from -0.09375 to 0.09375
- value_weight: bfloat16 [4096, 4096], P('kv', 'tp'), may hold values from -0.09375 to 0.09375
- output_gate_weight: bfloat16 [4096, 4096], P('kv', 'tp'), may hold values from -0.09375 to 0.09375
- lowrank_weight: bfloat16 [4096, 16], replicated, may hold values from -0.09375 to 0.09375
- decay_weight: bfloat16 [16, 2048], replicated, may hold values from -1.5 to 1.5
- decay_preact_bias: float32 [2048], replicated, may hold values from -1 to 20
- head_norm_gain: float32 [256], replicated, may hold values from 0.1 to 1.9
- output_weight: bfloat16 [4096, 4096], P('tp', 'kv'), may hold values from -0.1875 to 0.1875
- feedforward_norm_gain: float32 [4096], replicated, may hold values from 0.1 to 1.9
- feedforward_gate_weight: bfloat16 [4096, 10240], P('kv', 'tp'), may hold values from -0.09375 to 0.09375
- feedforward_up_weight: bfloat16 [4096, 10240], P('kv', 'tp'), may hold values from -0.09375 to 0.09375
- feedforward_down_weight: bfloat16 [10240, 4096], P('tp', 'kv'), may hold values from -0.109375 to 0.109375
- past_key_cache: bfloat16 [24, 6144, 2048], P(None, 'kv', 'tp'), may hold values from -6 to 6
- past_value_cache: bfloat16 [24, 6144, 4096], P(None, 'kv', 'tp'), may hold values from -6 to 6
- past_lowrank_cache: bfloat16 [24, 16, 6144], P(None, None, 'kv'), may hold values from -8 to 8
- head_extra_decay: float32 [24, 16, 6144], P(None, 'tp', 'kv'), may hold values from -0.7 to 0
- lengths: int32 [24], replicated, may hold values from 1 to 6144, 41472 in all
Outputs:
- output: bfloat16 [24, 4096], P(None, 'kv')
All inputs are finite; a program needn't handle non-finite values.
Results may differ from a plain program's by a relative error of at most 0.0085.
Values may be sent and summed in bfloat16 or wider, within the bound.
No kernel may reach another device: no remote copies, remote signals or barrier semaphores. Data moves between devices by JAX's collectives and lax.ppermute only.
A program may use at most 64 MiB of HBM per device.

v0:
```python
import functools

import jax
import jax.numpy as jnp
from jax import lax
from jax.sharding import Mesh
from jax.sharding import PartitionSpec as P

D = 4096
KEY_CHANNELS = 128
DV = 256
BLOCK = 64
TP = ("tp_0", "tp_1")


NORM_EPSILON = 1e-06


def rows_for(lines, size):
    spare = -lines.shape[0] % size
    if not spare:
        return lines
    return jnp.concatenate([lines, jnp.zeros((spare, *lines.shape[1:]), lines.dtype)])


def sent_to_all(array, axis):
    copies = jnp.broadcast_to(array, (lax.axis_size(axis), *array.shape))
    return lax.all_to_all(copies, axis, split_axis=0, concat_axis=0, tiled=True)


def in_order(pieces, dim):
    pieces = jnp.moveaxis(pieces, 0, dim)
    shape = pieces.shape
    return pieces.reshape(*shape[:dim], shape[dim] * shape[dim + 1], *shape[dim + 2 :])


def gather_directly(array, axis, dim):
    pieces = sent_to_all(array, axis)
    return in_order(pieces, dim)


def in_blocks(array, dim, size):
    shape = array.shape
    pieces = array.reshape(*shape[:dim], size, shape[dim] // size, *shape[dim + 1 :])
    return jnp.moveaxis(pieces, dim, 0)


def summed_on_arrival(array, axis, dim):
    size = lax.axis_size(axis)
    pieces = lax.all_to_all(in_blocks(array, dim, size), axis, 0, 0, tiled=True)
    return jnp.sum(pieces, axis=0)


def total_of(array, axes):
    padded = rows_for(array, lax.axis_size(axes))
    whole = gather_directly(summed_on_arrival(padded, axes, 0), axes, 0)
    return lax.slice_in_dim(whole, 0, len(array)).reshape(array.shape)


def packed_total(arrays, axis):
    ends = [0]
    for a in arrays:
        ends.append(ends[-1] + a.size)
    so_far = total_of(jnp.concatenate([a.ravel() for a in arrays]), axis)
    return tuple((so_far[b:e].reshape(a.shape) for a, b, e in zip(arrays, ends, ends[1:])))


def combined_pairwise(pieces, combine):
    while len(jax.tree.leaves(pieces)[0]) > 1:
        pieces = jax.vmap(combine)(*(pieces[side::2] for side in (0, 1)))
    return pieces[0]


def entering(array, axis, combine, identity):
    size, position = (lax.axis_size(axis), lax.axis_index(axis))
    passed = jnp.arange(size) > position

    def kept(part, zero, own):
        part = jnp.where(
            passed.reshape(-1, *(1 for _ in own.shape)), part, jnp.asarray(zero, own.dtype)
        )
        return part[::-1]

    pieces = sent_to_all(array, axis)
    return combined_pairwise(kept(pieces, identity, array), combine)


def taken_together(array, axis):
    return sent_to_all(array, axis).sum(axis=0)


def one_axis_at_a_time(array, axes):
    return functools.reduce(lax.psum, axes, array)


def product(operand, weights):
    return jnp.dot(operand, weights, preferred_element_type=jnp.float32)


def upper_ones(extent):
    row_ids = lax.broadcasted_iota(jnp.int32, (extent, extent), 0)
    col_ids = lax.broadcasted_iota(jnp.int32, (extent, extent), 1)
    return (col_ids > row_ids).astype(jnp.float32)


def add_totals(earlier, later_part):
    return earlier + later_part


def shards(
    tokens,
    attention_norm_gain,
    query_weight,
    key_weight,
    value_weight,
    output_gate_weight,
    lowrank_weight,
    decay_weight,
    decay_preact_bias,
    head_norm_gain,
    output_weight,
    feedforward_norm_gain,
    feedforward_gate_weight,
    feedforward_up_weight,
    feedforward_down_weight,
    past_key_cache,
    past_value_cache,
    past_lowrank_cache,
    head_extra_decay,
    lengths,
):
    sequences, row_width = tokens.shape
    kv_index = lax.axis_index("kv")
    tp_index = lax.axis_index(TP)
    channels = query_weight.shape[1]
    device_heads = head_extra_decay.shape[1]
    positions = past_key_cache.shape[1]
    block_count = positions // BLOCK
    row_start = kv_index * row_width
    rows_float = tokens.astype(jnp.float32)
    gain_one = lax.dynamic_slice_in_dim(attention_norm_gain, row_start, row_width)
    scaled = (rows_float * gain_one).astype(jnp.bfloat16)
    low_rows = lax.dynamic_slice_in_dim(lowrank_weight, row_start, row_width, 0)
    projected = packed_total(
        (
            jnp.sum(rows_float * rows_float, axis=1),
            product(scaled, query_weight),
            product(scaled, key_weight),
            product(scaled, value_weight),
            product(scaled, output_gate_weight),
            product(scaled, low_rows),
        ),
        "kv",
    )
    sq_total, query_part, key_part, value_part, outgate_part, lowrank_part = projected
    inv_rms = lax.rsqrt(sq_total / D + NORM_EPSILON)[:, None]
    query_vector = (inv_rms * query_part).astype(jnp.bfloat16)
    fresh_key = (inv_rms * key_part).astype(jnp.bfloat16)
    fresh_value = (inv_rms * value_part).astype(jnp.bfloat16)
    outgate = (inv_rms * outgate_part).astype(jnp.bfloat16)
    lowrank = (inv_rms * lowrank_part).astype(jnp.bfloat16)
    chan_start = tp_index * channels
    decay_cols = lax.dynamic_slice_in_dim(decay_weight, chan_start, channels, 1)
    bias_cols = lax.dynamic_slice_in_dim(decay_preact_bias, chan_start, channels)
    fresh_gate_value = jax.nn.log_sigmoid(product(lowrank, decay_cols) + bias_cols) / 16.0
    pre_cache = (
        jnp.einsum(
            "srp,rc->spc", past_lowrank_cache, decay_cols, preferred_element_type=jnp.float32
        )
        + bias_cols
    )
    gate_cache = jax.nn.log_sigmoid(pre_cache) / 16.0
    gate_cache = (
        gate_cache.reshape(sequences, positions, device_heads, KEY_CHANNELS)
        + jnp.transpose(head_extra_decay, (0, 2, 1))[..., None]
    )
    position_ids = kv_index * positions + lax.broadcasted_iota(jnp.int32, (sequences, positions), 1)
    is_live = position_ids < lengths[:, None]
    gate_cache = jnp.where(is_live[:, :, None, None], gate_cache, 0.0).reshape(
        sequences, block_count, BLOCK, channels
    )
    inside = jnp.einsum("ij,snjc->snic", upper_ones(BLOCK), gate_cache)
    block_totals = jnp.sum(gate_cache, axis=2)
    after_blocks = jnp.einsum("mn,snc->smc", upper_ones(block_count), block_totals)
    local_total = jnp.sum(block_totals, axis=1)
    later_sum = entering(local_total, "kv", add_totals, jnp.zeros_like(local_total))
    carried = after_blocks + later_sum[:, None, :] + fresh_gate_value[:, None, :]
    weighting = jnp.exp(inside + carried[:, :, None, :]).reshape(sequences, positions, channels)
    query_scaled = query_vector.astype(jnp.float32) * KEY_CHANNELS ** (-0.5)
    products = past_key_cache.astype(jnp.float32) * weighting * query_scaled[:, None, :]
    scores = jnp.sum(products.reshape(sequences, positions, device_heads, KEY_CHANNELS), axis=3)
    scores = jnp.where(is_live[:, :, None], scores, 0.0).astype(jnp.bfloat16)
    partial_out = jnp.einsum(
        "sph,sphv->shv",
        scores,
        past_value_cache.reshape(sequences, positions, device_heads, DV),
        preferred_element_type=jnp.float32,
    )
    summed = taken_together(partial_out, "kv")
    own_score = jnp.sum(
        (query_scaled * fresh_key.astype(jnp.float32)).reshape(
            sequences, device_heads, KEY_CHANNELS
        ),
        axis=2,
    )
    mixer_output = summed + own_score[:, :, None] * fresh_value.astype(jnp.float32).reshape(
        sequences, device_heads, DV
    )
    mean_sq = jnp.mean(mixer_output * mixer_output, axis=2, keepdims=True)
    gate_act = jax.nn.silu(outgate.astype(jnp.float32).reshape(sequences, device_heads, DV))
    gated = (mixer_output * lax.rsqrt(mean_sq + NORM_EPSILON) * head_norm_gain * gate_act).astype(
        jnp.bfloat16
    )
    attn_rows = one_axis_at_a_time(
        product(gated.reshape(sequences, device_heads * DV), output_weight), TP
    )
    residual = rows_float + attn_rows
    gain_two = lax.dynamic_slice_in_dim(feedforward_norm_gain, row_start, row_width)
    scaled_two = (residual * gain_two).astype(jnp.bfloat16)
    square_two = jnp.sum(residual * residual, axis=1)
    sq_sum, gate_sum, up_sum = packed_total(
        (
            square_two,
            product(scaled_two, feedforward_gate_weight),
            product(scaled_two, feedforward_up_weight),
        ),
        "kv",
    )
    inv_two = lax.rsqrt(sq_sum / D + NORM_EPSILON)[:, None]
    hidden = (jax.nn.silu(inv_two * gate_sum) * (inv_two * up_sum)).astype(jnp.bfloat16)
    down_part = product(hidden, feedforward_down_weight)
    mlp_rows = one_axis_at_a_time(down_part, TP)
    return (residual + mlp_rows).astype(jnp.bfloat16)


def solution(mesh):
    finer = Mesh(mesh.devices.reshape(mesh.shape["kv"], 4, 4), ("kv", "tp_0", "tp_1"))
    placed = (
        P(None, "kv"),
        P(),
        P("kv", TP),
        P("kv", TP),
        P("kv", TP),
        P("kv", TP),
        P(),
        P(),
        P(),
        P(),
        P(TP, "kv"),
        P(),
        P("kv", TP),
        P("kv", TP),
        P(TP, "kv"),
        P(None, "kv", TP),
        P(None, "kv", TP),
        P(None, None, "kv"),
        P(None, TP, "kv"),
        P(),
    )
    return jax.shard_map(
        shards, mesh=finer, in_specs=placed, out_specs=P(None, "kv"), check_vma=False
    )
```

profile of v0, /device:TPU:8, one launch (start us, length us, event | category | flops | bytes accessed | tf_op | source)
XLA Modules:
  0.0 251.1 jit_solution(6380743134468732380)
XLA Ops:
  0.0 1.0 fusion.21
  3.5 0.9 convolution_bitcast_fusion.3
  4.4 1.0 convolution_bitcast_fusion.1
  5.5 1.0 convolution_bitcast_fusion
  7.4 15.5 %all-to-all-start.1 = ((f32[32,1,589]{2,1,0:T(1,128)}), f32[32,1,589]{2,1,0:T(1,128)S(1)}, u32[]{:S(2)}, u32[]{:S(2)}) async-start(f32[32,1,589]{2,1,0:T(1,128)} %all_to_all.27), calls=%async_computation.1 | async-start | bytes 163840 | tf_op jit(solution)/shard_map/all_to_all | solution.py:50
  25.1 12.8 %all-to-all-done.1 = f32[32,1,589]{2,1,0:T(1,128)S(1)} async-done(((f32[32,1,589]{2,1,0:T(1,128)}), f32[32,1,589]{2,1,0:T(1,128)S(1)}, u32[]{:S(2)}, u32[]{:S(2)}) %all-to-all-start.1) | async-done | bytes 75424 | tf_op jit(solution)/shard_map/all_to_all | solution.py:50
  38.7 3.9 %all-to-all-start.2 = ((f32[32,1,589]{2,1,0:T(1,128)}), f32[32,1,589]{2,1,0:T(1,128)S(1)}, u32[]{:S(2)}, u32[]{:S(2)}) async-start(f32[32,1,589]{2,1,0:T(1,128)} %broadcast_in_dim.60), calls=%async_computation.2 | async-start | bytes 163840 | tf_op jit(solution)/shard_map/all_to_all | solution.py:28
  42.6 4.3 %fusion.58 = (f32[24,128]{1,0:T(8,128)S(1)}, f32[24,192,128]{2,1,0:T(8,128)}) fusion(f32[24,192]{1,0:T(8,128)S(1)} %bitcast.96, f32[128]{0:T(128)S(1)} %dynamic_slice.16, bf16[24,16,192]{2,1,0:T(8,128)(2,1)} %param.37, bf16[16,2048]{1,0:T(8,128)(2,1)} %param.27, s32[]{:T(128)S(6)} %select_n.35, pred[24,192]{1,0:T(8,128)(4,1)S(1)} %broadcast_compare_fusion), kind=kOutput, calls=%fused_computation.99 | convolution fusion | flops 26539008 | bytes 2595844 | tf_op jit(solution)/shard_map/srp,rc->spc/dot_general | solution.py:167
  46.9 10.8 %all-to-all-done.2 = f32[32,1,589]{2,1,0:T(1,128)S(1)} async-done(((f32[32,1,589]{2,1,0:T(1,128)}), f32[32,1,589]{2,1,0:T(1,128)S(1)}, u32[]{:S(2)}, u32[]{:S(2)}) %all-to-all-start.2) | async-done | bytes 75424 | tf_op jit(solution)/shard_map/all_to_all | solution.py:28
  58.4 3.9 %all-to-all-start = ((f32[32,24,128]{2,1,0:T(8,128)}), f32[32,24,128]{2,1,0:T(8,128)S(1)}, u32[]{:S(2)}, u32[]{:S(2)}) async-start(f32[32,24,128]{2,1,0:T(8,128)} %broadcast_in_dim.58), calls=%async_computation | async-start | bytes 786432 | tf_op jit(solution)/shard_map/all_to_all | solution.py:28
  62.3 2.0 reduce_sum.90
  64.9 0.9 fusion.25
  65.8 24.9 %all-to-all-done = f32[32,24,128]{2,1,0:T(8,128)S(1)} async-done(((f32[32,24,128]{2,1,0:T(8,128)}), f32[32,24,128]{2,1,0:T(8,128)S(1)}, u32[]{:S(2)}, u32[]{:S(2)}) %all-to-all-start) | async-done | bytes 393248 | tf_op jit(solution)/shard_map/all_to_all | solution.py:28
  91.0 1.3 copy-done.1
  95.4 0.9 broadcast_in_dim.63
  96.3 3.9 %all-to-all-start.3 = ((f32[32,24,1,256]{3,1,2,0:T(8,128)}), f32[32,24,1,256]{3,1,2,0:T(8,128)S(1)}, u32[]{:S(2)}, u32[]{:S(2)}) async-start(f32[32,24,1,256]{3,1,2,0:T(8,128)} %broadcast_in_dim.63), calls=%async_computation.3 | async-start | bytes 1572864 | tf_op jit(solution)/shard_map/all_to_all | solution.py:28
  101.3 44.2 %all-to-all-done.3 = f32[32,24,1,256]{3,1,2,0:T(8,128)S(1)} async-done(((f32[32,24,1,256]{3,1,2,0:T(8,128)}), f32[32,24,1,256]{3,1,2,0:T(8,128)S(1)}, u32[]{:S(2)}, u32[]{:S(2)}) %all-to-all-start.3) | async-done | bytes 786464 | tf_op jit(solution)/shard_map/all_to_all | solution.py:28
  145.9 14.1 %psum.28 = f32[24,128]{1,0:T(8,128)S(1)} all-reduce(f32[24,128]{1,0:T(8,128)S(1)} %fusion.31), channel_id=1, replica_groups=mesh['kv'=32,'tp_0'=4,'tp_1'=4] {'tp_0'}, use_global_device_ids=true, to_apply=%region_8.9 | all-reduce | flops 3072 | bytes 24576 | tf_op jit(solution)/shard_map/psum | solution.py:93
  160.0 16.8 %psum.29 = f32[24,128]{1,0:T(8,128)S(1)} all-reduce(f32[24,128]{1,0:T(8,128)S(1)} %psum.28), channel_id=1, replica_groups=mesh['kv'=32,'tp_0'=4,'tp_1'=4] {'tp_1'}, use_global_device_ids=true, to_apply=%region_9.10 | all-reduce | flops 3072 | bytes 24576 | tf_op jit(solution)/shard_map/psum | solution.py:93
  177.1 1.1 fusion.59
  178.5 20.1 %all_to_all.40 = f32[32,1,961]{2,1,0:T(1,128)S(1)} all-to-all(f32[32,1,961]{2,1,0:T(1,128)S(1)} %all_to_all.31), channel_id=1, replica_groups=mesh['kv'=32,'tp_0'=4,'tp_1'=4] {'kv'}, dimensions={0} | all-to-all | bytes 246016 | tf_op jit(solution)/shard_map/all_to_all | solution.py:50
  198.9 20.1 %all_to_all.41 = f32[32,1,961]{2,1,0:T(1,128)S(1)} all-to-all(f32[32,1,961]{2,1,0:T(1,128)S(1)} %broadcast_in_dim.64), channel_id=1, replica_groups=mesh['kv'=32,'tp_0'=4,'tp_1'=4] {'kv'}, dimensions={0} | all-to-all | bytes 246016 | tf_op jit(solution)/shard_map/all_to_all | solution.py:28
  219.9 16.4 %psum.30 = f32[24,128]{1,0:T(8,128)S(1)} all-reduce(f32[24,128]{1,0:T(8,128)S(1)} %fusion.13), channel_id=1, replica_groups=mesh['kv'=32,'tp_0'=4,'tp_1'=4] {'tp_0'}, use_global_device_ids=true, to_apply=%region_12.13 | all-reduce | flops 3072 | bytes 24576 | tf_op jit(solution)/shard_map/psum | solution.py:93
  236.2 14.3 %psum.31 = f32[24,128]{1,0:T(8,128)S(1)} all-reduce(f32[24,128]{1,0:T(8,128)S(1)} %psum.30), channel_id=1, replica_groups=mesh['kv'=32,'tp_0'=4,'tp_1'=4] {'tp_1'}, use_global_device_ids=true, to_apply=%region_13.14 | all-reduce | flops 3072 | bytes 24576 | tf_op jit(solution)/shard_map/psum | solution.py:93
  (79 shorter events, 14.8 us)
Async XLA Ops:
  0.0 94.9 %copy-start = (bf16[24,192,256]{2,1,0:T(8,128)(2,1)S(1)}, bf16[24,192,256]{2,1,0:T(8,128)(2,1)}, u32[]{:S(2)}) copy-start(bf16[24,192,256]{2,1,0:T(8,128)(2,1)} %param.36) | copy-start | bytes 7077892
  7.4 30.6 %all-to-all-start.1 = ((f32[32,1,589]{2,1,0:T(1,128)}), f32[32,1,589]{2,1,0:T(1,128)S(1)}, u32[]{:S(2)}, u32[]{:S(2)}) async-start(f32[32,1,589]{2,1,0:T(1,128)} %all_to_all.27), calls=%async_computation.1 | async-start | bytes 163840 | tf_op jit(solution)/shard_map/all_to_all | solution.py:50
  38.7 18.9 %all-to-all-start.2 = ((f32[32,1,589]{2,1,0:T(1,128)}), f32[32,1,589]{2,1,0:T(1,128)S(1)}, u32[]{:S(2)}, u32[]{:S(2)}) async-start(f32[32,1,589]{2,1,0:T(1,128)} %broadcast_in_dim.60), calls=%async_computation.2 | async-start | bytes 163840 | tf_op jit(solution)/shard_map/all_to_all | solution.py:28
  58.4 32.2 %all-to-all-start = ((f32[32,24,128]{2,1,0:T(8,128)}), f32[32,24,128]{2,1,0:T(8,128)S(1)}, u32[]{:S(2)}, u32[]{:S(2)}) async-start(f32[32,24,128]{2,1,0:T(8,128)} %broadcast_in_dim.58), calls=%async_computation | async-start | bytes 786432 | tf_op jit(solution)/shard_map/all_to_all | solution.py:28
  90.7 1.7 copy-start.1
  92.3 1.3 copy-start.2
  93.9 0.9 copy-start.5
  95.3 50.4 %copy-start.7 = (bf16[256,128]{1,0:T(8,128)(2,1)S(1)}, bf16[256,128]{1,0:T(8,128)(2,1)}, u32[]{:S(2)}) copy-start(bf16[256,128]{1,0:T(8,128)(2,1)} %param.30) | copy-start | bytes 196612
  95.3 50.4 %copy-start.8 = (f32[256]{0:T(256)S(1)}, f32[256]{0:T(256)}, u32[]{:S(2)}) copy-start(f32[256]{0:T(256)} %param.29) | copy-start | bytes 3076
  95.3 81.5 %copy-start.3 = (bf16[24,128]{1,0:T(8,128)(2,1)S(1)}, bf16[24,128]{1,0:T(8,128)(2,1)}, u32[]{:S(2)}) copy-start(bf16[24,128]{1,0:T(8,128)(2,1)} %param.20) | copy-start | bytes 18436
  95.3 81.6 %copy-start.4 = (bf16[128,640]{1,0:T(8,128)(2,1)S(1)}, bf16[128,640]{1,0:T(8,128)(2,1)}, u32[]{:S(2)}) copy-start(bf16[128,640]{1,0:T(8,128)(2,1)} %param.33) | copy-start | bytes 491524
  96.3 49.2 %all-to-all-start.3 = ((f32[32,24,1,256]{3,1,2,0:T(8,128)}), f32[32,24,1,256]{3,1,2,0:T(8,128)S(1)}, u32[]{:S(2)}, u32[]{:S(2)}) async-start(f32[32,24,1,256]{3,1,2,0:T(8,128)} %broadcast_in_dim.63), calls=%async_computation.3 | async-start | bytes 1572864 | tf_op jit(solution)/shard_map/all_to_all | solution.py:28
  145.5 74.1 %copy-start.6 = (bf16[640,128]{1,0:T(8,128)(2,1)S(1)}, bf16[640,128]{1,0:T(8,128)(2,1)}, u32[]{:S(2)}) copy-start(bf16[640,128]{1,0:T(8,128)(2,1)} %param.34) | copy-start | bytes 491524
where the time goes:
time: 252 us; the launch traced here: 251 us
  blocking collectives  102 us (40%)
  waiting for transfers between devices  92.7 us (37%)
  starting transfers between devices  27.1 us (11%)
  matrix products  12.5 us (5%)
  local copies, waits for them, and re-layouts  9.65 us (4%)
  other arithmetic  7.01 us (3%)
    all_to_all x3, waiting for transfers between devices, sent_to_all(): return lax.all_to_all(copies, axis, split_axis=0, concat_axis=0, tiled=True)  79.8 us
    psum x4, blocking collectives, one_axis_at_a_time(): return functools.reduce(lax.psum, axes, array)  61.5 us
    all_to_all x1, blocking collectives, summed_on_arrival(): pieces = lax.all_to_all(in_blocks(array, dim, size), axis, 0, 0, tiled=True)  20.1 us
    all_to_all x1, blocking collectives, sent_to_all(): return lax.all_to_all(copies, axis, split_axis=0, concat_axis=0, tiled=True)  20.1 us
    all_to_all x1, starting transfers between devices, summed_on_arrival(): pieces = lax.all_to_all(in_blocks(array, dim, size), axis, 0, 0, tiled=True)  15.5 us
    all_to_all x1, waiting for transfers between devices, summed_on_arrival(): pieces = lax.all_to_all(in_blocks(array, dim, size), axis, 0, 0, tiled=True)  12.8 us
    all_to_all x3, starting transfers between devices, sent_to_all(): return lax.all_to_all(copies, axis, split_axis=0, concat_axis=0, tiled=True)  11.6 us
    dot_general x10, matrix products, product(): return jnp.dot(operand, weights, preferred_element_type=jnp.float32)  7.17 us
  transfers between devices with their start and end apart: 4, of which 4 were waited for; matrix products, arithmetic and copies ran while one was open for 4% of the time, Pallas kernels for 0%

commit v1 on v0

v1 whole, which is shorter than its diff:
```python
import jax
import jax.numpy as jnp
from jax import lax
from jax.sharding import Mesh
from jax.sharding import PartitionSpec as P

D = 4096
KEY_CHANNELS = 128
DV = 256
GROUPS = 8
MEMBERS = 4
OWN = 6
KV = ("kvh", "kvl")
TP = ("tp_0", "tp_1")
NORM_EPSILON = 1e-06
BF = jnp.bfloat16
F32 = jnp.float32


def exchange(array, axes):
    return lax.all_to_all(array, axes, split_axis=0, concat_axis=0, tiled=True)


def product(operand, weights):
    return jnp.dot(operand, weights, preferred_element_type=F32)


def copies(array, size):
    return jnp.broadcast_to(array, (size, *array.shape))


def split_two(array):
    high = array.astype(BF)
    low = (array - high.astype(F32)).astype(BF)
    return high.astype(F32), low.astype(F32)


def log_gate(values):
    return (jnp.minimum(values, 0.0) - jnp.log(1.0 + jnp.exp(-jnp.abs(values)))) / 16.0


def by_owner(rows):
    rest = rows.shape[1:]
    grid = jnp.swapaxes(rows.reshape(MEMBERS, OWN, *rest), 0, 1)
    pad = jnp.zeros((GROUPS - OWN, MEMBERS, *rest), rows.dtype)
    return jnp.concatenate([grid, pad]).reshape(GROUPS * MEMBERS, *rest)


def shards(
    tokens,
    attention_norm_gain,
    query_weight,
    key_weight,
    value_weight,
    output_gate_weight,
    lowrank_weight,
    decay_weight,
    decay_preact_bias,
    head_norm_gain,
    output_weight,
    feedforward_norm_gain,
    feedforward_gate_weight,
    feedforward_up_weight,
    feedforward_down_weight,
    past_key_cache,
    past_value_cache,
    past_lowrank_cache,
    head_extra_decay,
    lengths,
):
    sequences, width = tokens.shape
    group, member = lax.axis_index("kvh"), lax.axis_index("kvl")
    place = group * MEMBERS + member
    head = lax.axis_index(TP)
    positions = past_key_cache.shape[1]
    row_start = place * width
    tokens_f = tokens.astype(F32)
    gain_one = lax.dynamic_slice_in_dim(attention_norm_gain, row_start, width)
    scaled = (tokens_f * gain_one).astype(BF)
    low_rows = lax.dynamic_slice_in_dim(lowrank_weight, row_start, width, 0)
    squares = jnp.sum(tokens_f * tokens_f, axis=1)
    decay_cols = lax.dynamic_slice_in_dim(decay_weight, head * KEY_CHANNELS, KEY_CHANNELS, 1)
    bias_cols = lax.dynamic_slice_in_dim(decay_preact_bias, head * KEY_CHANNELS, KEY_CHANNELS)
    pre = jnp.einsum("srp,rc->spc", past_lowrank_cache, decay_cols, preferred_element_type=F32)
    gates = log_gate(pre + bias_cols) + jnp.transpose(head_extra_decay, (0, 2, 1))
    ids = place * positions + lax.broadcasted_iota(jnp.int32, (sequences, positions), 1)
    live = (ids < lengths[:, None])[:, :, None]
    gates = jnp.where(live, gates, 0.0)
    totals = jnp.sum(gates, axis=1)
    sq_high, sq_low = split_two(squares)
    low_row = jnp.concatenate(
        [
            product(scaled, low_rows).reshape(MEMBERS, 96),
            sq_high.reshape(MEMBERS, OWN),
            sq_low.reshape(MEMBERS, OWN),
            jnp.zeros((MEMBERS, 20), F32),
        ],
        axis=1,
    )[:, None, :]
    shared = jnp.concatenate(
        [
            product(scaled, query_weight).reshape(MEMBERS, OWN, KEY_CHANNELS),
            totals.reshape(MEMBERS, OWN, KEY_CHANNELS),
            low_row,
        ],
        axis=1,
    )
    owned = by_owner(
        jnp.concatenate(
            [
                product(scaled, key_weight)[:, None, :],
                product(scaled, value_weight).reshape(sequences, 2, 128),
                product(scaled, output_gate_weight).reshape(sequences, 2, 128),
            ],
            axis=1,
        )
    )
    first = jnp.concatenate(
        [copies(shared, GROUPS).reshape(32, 13, 128), owned], axis=1
    ).astype(BF)
    got = exchange(first.reshape(32, 9, 2, 128), KV).reshape(32, 18, 128).astype(F32)
    order = lax.broadcasted_iota(jnp.int32, (positions, positions), 0)
    later_ones = (lax.broadcasted_iota(jnp.int32, (positions, positions), 1) > order).astype(BF)
    high = gates.astype(BF)
    low = (gates - high.astype(F32)).astype(BF)
    suffix = jnp.einsum("ij,sjc->sic", later_ones, high, preferred_element_type=F32) + jnp.einsum(
        "ij,sjc->sic", later_ones, low, preferred_element_type=F32
    )
    weighted = jnp.where(live, past_key_cache.astype(F32) * jnp.exp(suffix), 0.0).astype(BF)
    state = jnp.einsum(
        "spc,spv->scv", weighted, past_value_cache, preferred_element_type=F32
    ).astype(BF)
    sums = jnp.sum(got, axis=0)
    later_totals = got[:, OWN : 2 * OWN]
    inv = lax.rsqrt((sums[12, 96:102] + sums[12, 102:108]) / D + NORM_EPSILON)[:, None]
    query = (inv * sums[:OWN]).astype(BF).astype(F32) * KEY_CHANNELS ** (-0.5)
    lowrank = (inv * sums[12, :96].reshape(OWN, 16)).astype(BF)
    fresh = log_gate(product(lowrank, decay_cols) + bias_cols)
    ends = group * MEMBERS + jnp.arange(MEMBERS)
    after = (jnp.arange(32)[None, :] > ends[:, None]).astype(F32)
    later = jnp.sum(after[:, :, None, None] * later_totals[None], axis=1)
    ready = query * jnp.exp(fresh + later)
    ready = jnp.concatenate([ready, jnp.zeros((MEMBERS, 2, 128), F32)], axis=1)
    mine = (jnp.arange(OWN) == group).astype(F32)[:, None]
    own_inv = jnp.sum(mine * inv)
    key_new = (own_inv * sums[13]).astype(BF).astype(F32)
    value_new = (own_inv * sums[14:16].reshape(DV)).astype(BF).astype(F32)
    outgate = (own_inv * sums[16:18].reshape(DV)).astype(BF)
    own_value = jnp.sum(jnp.sum(mine * query, axis=0) * key_new) * value_new
    whole = exchange(ready, "kvl")[:, :OWN].reshape(sequences, KEY_CHANNELS)
    part = jnp.einsum("sc,scv->sv", whole, state.astype(F32))
    at_own = (jnp.arange(sequences) == member * OWN + group) & (group < OWN)
    part = part + jnp.where(at_own[:, None], own_value[None, :], 0.0)
    second = jnp.concatenate(
        [
            part.reshape(MEMBERS, OWN, DV).astype(BF),
            jnp.broadcast_to(outgate, (MEMBERS, 2, DV)),
        ],
        axis=1,
    )
    second = copies(second, GROUPS).reshape(32, 8, DV)
    back = exchange(second, KV)
    mixed = jnp.sum(back[:, :OWN].astype(F32), axis=0)
    outgates = lax.dynamic_index_in_dim(
        back.reshape(GROUPS, MEMBERS, 8, DV)[:OWN, :, OWN], member, 1, keepdims=False
    ).astype(F32)
    mean_sq = jnp.mean(mixed * mixed, axis=1, keepdims=True)
    gated = (
        mixed * lax.rsqrt(mean_sq + NORM_EPSILON) * head_norm_gain * jax.nn.silu(outgates)
    ).astype(BF)
    columns = exchange(copies(output_weight, MEMBERS), "kvl")
    rows = jnp.einsum("sv,rvc->rsc", gated, columns, preferred_element_type=F32).astype(BF)
    rows = jnp.concatenate([rows, jnp.zeros((MEMBERS, 2, 128), BF)], axis=1)
    rows = jnp.broadcast_to(rows[:, None], (MEMBERS, 16, 8, 128)).reshape(64, 8, 128)
    rows = exchange(rows, ("kvl", *TP)).reshape(MEMBERS, 16, 8, 128)
    attention = jnp.sum(rows[:, :, :OWN].astype(F32), axis=1).reshape(sequences, width)
    residual = tokens_f + attention
    gain_two = lax.dynamic_slice_in_dim(feedforward_norm_gain, row_start, width)
    scaled_two = (residual * gain_two).astype(BF)
    square_parts = jnp.stack(split_two(jnp.sum(residual * residual, axis=1)), axis=1)
    wide = jnp.stack(
        [
            product(scaled_two, feedforward_gate_weight),
            product(scaled_two, feedforward_up_weight),
        ],
        axis=1,
    )
    units = wide.shape[2]
    third = jnp.concatenate(
        [wide, jnp.broadcast_to(square_parts[:, :, None], (sequences, 2, 128))], axis=2
    )
    third = exchange(by_owner(third).astype(BF), KV)
    sums_two = jnp.sum(third.astype(F32), axis=0)
    inv_two = lax.rsqrt((sums_two[0, units] + sums_two[1, units]) / D + NORM_EPSILON)
    hidden = (
        jax.nn.silu(inv_two * sums_two[0, :units]) * (inv_two * sums_two[1, :units])
    ).astype(BF)
    hidden = jnp.concatenate([hidden, jnp.zeros((1024 - units,), BF)]).reshape(8, 128)
    hidden = exchange(copies(hidden, 32), KV).reshape(GROUPS, MEMBERS, 1024)[:OWN, :, :units]
    hidden = jnp.swapaxes(hidden, 0, 1).reshape(sequences, units)
    down = product(hidden, feedforward_down_weight).astype(BF)
    down = exchange(copies(down, 16), TP)
    return (residual + jnp.sum(down.astype(F32), axis=0)).astype(BF)


def solution(mesh):
    finer = Mesh(mesh.devices.reshape(GROUPS, MEMBERS, 4, 4), (*KV, *TP))
    placed = (
        P(None, KV),
        P(),
        P(KV, TP),
        P(KV, TP),
        P(KV, TP),
        P(KV, TP),
        P(),
        P(),
        P(),
        P(),
        P(TP, KV),
        P(),
        P(KV, TP),
        P(KV, TP),
        P(TP, KV),
        P(None, KV, TP),
        P(None, KV, TP),
        P(None, None, KV),
        P(None, TP, KV),
        P(),
    )
    return jax.shard_map(
        shards, mesh=finer, in_specs=placed, out_specs=P(None, KV), check_vma=False
    )
```

time: 252 us -> 172 us (0.68)
  the two profiles are of different devices: /device:TPU:8 before, /device:TPU:2 now
where the time goes in v1:
time: 172 us; the launch traced here: 171 us
  blocking collectives  68.1 us (40%)
  starting transfers between devices  30.9 us (18%)
  waiting for transfers between devices  21 us (12%)
  matrix products  17.5 us (10%)
  other arithmetic  17.3 us (10%)
  local copies, waits for them, and re-layouts  14.2 us (8%)
  between operations  1.82 us (1%)
    all_to_all x4, blocking collectives, exchange(): return lax.all_to_all(array, axes, split_axis=0, concat_axis=0, tiled=True)  68.1 us
    all_to_all x4, starting transfers between devices, exchange(): return lax.all_to_all(array, axes, split_axis=0, concat_axis=0, tiled=True)  30.9 us
    all_to_all x4, waiting for transfers between devices, exchange(): return lax.all_to_all(array, axes, split_axis=0, concat_axis=0, tiled=True)  21 us
    dot_general x1, matrix products, shards(): jnp.einsum('ij,sjc->sic', later_ones, low, preferred_element_type=F32)  4.19 us
    dot_general x1, matrix products, shards(): jnp.einsum('srp,rc->spc', past_lowrank_cache, decay_cols, preferred_eleme...  4.08 us
    dot_general x1, matrix products, shards(): jnp.einsum('ij,sjc->sic', later_ones, high, preferred_element_type=F32)  3.52 us
  transfers between devices with their start and end apart: 4, of which 4 were waited for; matrix products, arithmetic and copies ran while one was open for 8% of the time, Pallas kernels for 0%

profile of v1, /device:TPU:2, one launch (start us, length us, event | category | flops | bytes accessed | tf_op | source)
XLA Modules:
  0.0 170.9 jit_solution(5512451269942899846)
XLA Ops:
  5.0 4.1 %bitcast_reduce_fusion = (bf16[24,128]{1,0:T(8,128)(2,1)S(1)}, f32[128,24,192]{0,2,1:T(8,128)}) fusion(f32[24,192]{1,0:T(8,128)S(1)} %bitcast.145, f32[128]{0:T(128)S(1)} %dynamic_slice.21, bf16[24,16,192]{2,1,0:T(8,128)(2,1)} %param.37, bf16[16,2048]{1,0:T(8,128)(2,1)} %param.27, s32[]{:T(128)S(6)} %select_n.25, pred[24,192]{1,0:T(8,128)(4,1)S(1)} %broadcast_compare_fusion), kind=kOutput, calls=%fused_computation.5 | convolution fusion | flops 24769536 | bytes 2589700 | tf_op jit(solution)/shard_map/srp,rc->spc/dot_general | solution.py:84
  10.9 15.6 %all-to-all-start = ((bf16[32,9,2,128]{3,2,1,0:T(2,128)(2,1)}), bf16[32,9,2,128]{3,2,1,0:T(2,128)(2,1)}, u32[]{:S(2)}, u32[]{:S(2)}) async-start(bf16[32,9,2,128]{3,2,1,0:T(2,128)(2,1)} %copy.77), calls=%async_computation | async-start | bytes 294912 | tf_op jit(solution)/shard_map/all_to_all | solution.py:21
  27.2 3.5 %fusion.8 = f32[24,128,192]{1,2,0:T(8,128)} fusion(f32[128,24,192]{0,2,1:T(8,128)} %get-tuple-element.20), kind=kOutput, calls=%fused_computation.21 | convolution fusion | flops 226529280 | bytes 4718592 | tf_op jit(solution)/shard_map/ij,sjc->sic/dot_general | solution.py:126
  31.8 4.2 %fusion.1 = bf16[24,192,128]{2,1,0:T(8,128)(2,1)S(1)} fusion(f32[24,128,192]{1,2,0:T(8,128)} %fusion.8, bf16[24,192,128]{2,1,0:T(8,128)(2,1)} %param.35, f32[128,24,192]{0,2,1:T(8,128)} %get-tuple-element.20, pred[24,192]{1,0:T(8,128)(4,1)S(1)} %broadcast_compare_fusion), kind=kOutput, calls=%fused_computation.2 | convolution fusion | flops 231837696 | bytes 7082496 | tf_op jit(solution)/shard_map/ij,sjc->sic/dot_general | solution.py:126
  36.0 8.4 %all-to-all-done = bf16[32,9,2,128]{3,2,1,0:T(2,128)(2,1)} async-done(((bf16[32,9,2,128]{3,2,1,0:T(2,128)(2,1)}), bf16[32,9,2,128]{3,2,1,0:T(2,128)(2,1)}, u32[]{:S(2)}, u32[]{:S(2)}) %all-to-all-start) | async-done | bytes 147488 | tf_op jit(solution)/shard_map/all_to_all | solution.py:21
  44.4 1.6 convert_reduce_fusion
  46.0 1.3 reduce_sum.127
  49.1 2.1 %fusion.59 = (f32[6]{0:T(128)S(1)}, f32[1,6]{1,0:T(1,128)}) fusion(f32[]{:T(128)} %broadcast.198, f32[18,128]{1,0:T(8,128)} %reduce_sum.127), kind=kLoop, calls=%fused_computation.121 | loop fusion | flops 18 | bytes 100 | tf_op jit(solution)/shard_map/rsqrt | solution.py:135
  51.3 1.4 multiply_reduce_fusion.3
  53.4 1.3 fusion.47
  58.7 3.8 %all-to-all-start.1 = ((f32[4,8,128]{2,1,0:T(8,128)}), f32[4,8,128]{2,1,0:T(8,128)}, u32[]{:S(2)}, u32[]{:S(2)}) async-start(f32[4,8,128]{2,1,0:T(8,128)} %concatenate.51), calls=%async_computation.1 | async-start | bytes 32768 | tf_op jit(solution)/shard_map/all_to_all | solution.py:21
  62.6 1.9 %fusion.56 = f32[]{:T(128)} fusion(f32[128]{0:T(128)} %get-tuple-element.13, f32[18,128]{1,0:T(8,128)} %reduce_sum.127, f32[]{:T(128)} %fusion.47), kind=kLoop, calls=%fused_computation.119 | loop fusion | flops 639 | bytes 1032 | tf_op jit(solution)/shard_map/reduce_sum | solution.py:149
  64.5 1.9 %multiply_bitcast_fusion = (f32[256]{0:T(256)S(1)}, bf16[256]{0:T(256)(128)(2,1)S(1)}) fusion(f32[9,2,128]{2,1,0:T(2,128)} %convert_reduce_fusion, f32[]{:T(128)} %fusion.47, f32[]{:T(128)} %fusion.56), kind=kLoop, calls=%fused_computation.95 | loop fusion | flops 1536 | bytes 3592 | tf_op jit(solution)/shard_map/mul | solution.py:149
  66.5 1.3 reshape.280
  67.8 2.2 %fusion.3 = f32[24,1,256]{2,1,0:T(1,128)} fusion(f32[24,128,1]{1,2,0:T(1,128)} %bitcast.144, bf16[24,192,128]{2,1,0:T(8,128)(2,1)S(1)} %fusion.1, bf16[24,192,256]{2,1,0:T(8,128)(2,1)S(1)} %copy-done), kind=kOutput, calls=%fused_computation.9 | convolution fusion | flops 304349184 | bytes 3575808 | tf_op jit(solution)/shard_map/sc,scv->sv/dot_general | solution.py:151
  70.9 21.1 %all_to_all.40 = bf16[32,8,256]{2,1,0:T(8,128)(2,1)S(1)} all-to-all(bf16[32,8,256]{2,1,0:T(8,128)(2,1)S(1)} %bitcast.138), channel_id=1, replica_groups=mesh['kvh'=8,'kvl'=4,'tp_0'=4,'tp_1'=4] {'kvh','kvl'}, dimensions={0} | all-to-all | bytes 262144 | tf_op jit(solution)/shard_map/all_to_all | solution.py:21
  92.0 1.6 broadcast_in_dim.103
  93.6 3.4 %all-to-all-start.3 = ((bf16[4,256,128]{2,1,0:T(8,128)(2,1)}), bf16[4,256,128]{2,1,0:T(8,128)(2,1)S(1)}, u32[]{:S(2)}, u32[]{:S(2)}) async-start(bf16[4,256,128]{2,1,0:T(8,128)(2,1)} %broadcast_in_dim.103), calls=%async_computation.3 | async-start | bytes 524288 | tf_op jit(solution)/shard_map/all_to_all | solution.py:21
  97.2 5.7 %all-to-all-done.3 = bf16[4,256,128]{2,1,0:T(8,128)(2,1)S(1)} async-done(((bf16[4,256,128]{2,1,0:T(8,128)(2,1)}), bf16[4,256,128]{2,1,0:T(8,128)(2,1)S(1)}, u32[]{:S(2)}, u32[]{:S(2)}) %all-to-all-start.3) | async-done | bytes 262176 | tf_op jit(solution)/shard_map/all_to_all | solution.py:21
  104.5 8.0 %all-to-all-start.4 = ((bf16[64,8,128]{2,1,0:T(8,128)(2,1)}), bf16[64,8,128]{2,1,0:T(8,128)(2,1)S(1)}, u32[]{:S(2)}, u32[]{:S(2)}) async-start(bf16[64,8,128]{2,1,0:T(8,128)(2,1)} %bitcast.21), calls=%async_computation.4 | async-start | bytes 262144 | tf_op jit(solution)/shard_map/all_to_all | solution.py:21
  113.3 6.7 %all-to-all-done.4 = bf16[64,8,128]{2,1,0:T(8,128)(2,1)S(1)} async-done(((bf16[64,8,128]{2,1,0:T(8,128)(2,1)}), bf16[64,8,128]{2,1,0:T(8,128)(2,1)S(1)}, u32[]{:S(2)}, u32[]{:S(2)}) %all-to-all-start.4) | async-done | bytes 131104 | tf_op jit(solution)/shard_map/all_to_all | solution.py:21
  120.8 18.7 %all_to_all.41 = bf16[32,2,768]{2,1,0:T(2,128)(2,1)S(1)} all-to-all(bf16[32,2,768]{2,1,0:T(2,128)(2,1)S(1)} %bitcast.140), channel_id=1, replica_groups=mesh['kvh'=8,'kvl'=4,'tp_0'=4,'tp_1'=4] {'kvh','kvl'}, dimensions={0} | all-to-all | bytes 196608 | tf_op jit(solution)/shard_map/all_to_all | solution.py:21
  141.7 17.3 %all_to_all.42 = bf16[32,8,128]{2,1,0:T(8,128)(2,1)S(1)} all-to-all(bf16[32,8,128]{2,1,0:T(8,128)(2,1)S(1)} %broadcast_in_dim.106), channel_id=1, replica_groups=mesh['kvh'=8,'kvl'=4,'tp_0'=4,'tp_1'=4] {'kvh','kvl'}, dimensions={0} | all-to-all | bytes 131072 | tf_op jit(solution)/shard_map/all_to_all | solution.py:21
  159.2 11.0 %all_to_all.43 = bf16[16,24,128]{2,1,0:T(8,128)(2,1)S(1)} all-to-all(bf16[16,24,128]{2,1,0:T(8,128)(2,1)S(1)} %broadcast_in_dim.107), channel_id=1, replica_groups=mesh['kvh'=8,'kvl'=4,'tp_0'=4,'tp_1'=4] {'tp_0','tp_1'}, dimensions={0} | all-to-all | bytes 196608 | tf_op jit(solution)/shard_map/all_to_all | solution.py:21
  (111 shorter events, 20.9 us)
Async XLA Ops:
  0.0 67.8 %copy-start = (bf16[24,192,256]{2,1,0:T(8,128)(2,1)S(1)}, bf16[24,192,256]{2,1,0:T(8,128)(2,1)}, u32[]{:S(2)}) copy-start(bf16[24,192,256]{2,1,0:T(8,128)(2,1)} %param.36) | copy-start | bytes 7077892
  4.2 4.9 %copy-start.9 = (f32[128]{0:T(128)}, f32[128]{0:T(128)S(1)}, u32[]{:S(2)}) copy-start(f32[128]{0:T(128)S(1)} %dynamic_slice.21) | copy-start | bytes 1540
  5.0 4.2 %copy-start.1 = (bf16[24,128]{1,0:T(8,128)(2,1)S(1)}, bf16[24,128]{1,0:T(8,128)(2,1)}, u32[]{:S(2)}) copy-start(bf16[24,128]{1,0:T(8,128)(2,1)} %param.20) | copy-start | bytes 18436
  5.0 4.2 %copy-start.7 = (bf16[128,128]{1,0:T(8,128)(2,1)S(1)}, bf16[128,128]{1,0:T(8,128)(2,1)}, u32[]{:S(2)}) copy-start(bf16[128,128]{1,0:T(8,128)(2,1)} %param.22) | copy-start | bytes 98308
  5.0 4.3 %copy-start.5 = (bf16[128,256]{1,0:T(8,128)(2,1)S(1)}, bf16[128,256]{1,0:T(8,128)(2,1)}, u32[]{:S(2)}) copy-start(bf16[128,256]{1,0:T(8,128)(2,1)} %param.24) | copy-start | bytes 196612
  5.0 4.5 %copy-start.6 = (bf16[128,256]{1,0:T(8,128)(2,1)S(1)}, bf16[128,256]{1,0:T(8,128)(2,1)}, u32[]{:S(2)}) copy-start(bf16[128,256]{1,0:T(8,128)(2,1)} %param.25) | copy-start | bytes 196612
  5.0 4.7 %copy-start.8 = (bf16[128,128]{1,0:T(8,128)(2,1)S(1)}, bf16[128,128]{1,0:T(8,128)(2,1)}, u32[]{:S(2)}) copy-start(bf16[128,128]{1,0:T(8,128)(2,1)} %param.23) | copy-start | bytes 98308
  10.9 33.5 %all-to-all-start = ((bf16[32,9,2,128]{3,2,1,0:T(2,128)(2,1)}), bf16[32,9,2,128]{3,2,1,0:T(2,128)(2,1)}, u32[]{:S(2)}, u32[]{:S(2)}) async-start(bf16[32,9,2,128]{3,2,1,0:T(2,128)(2,1)} %copy.77), calls=%async_computation | async-start | bytes 294912 | tf_op jit(solution)/shard_map/all_to_all | solution.py:21
  58.7 7.8 %all-to-all-start.1 = ((f32[4,8,128]{2,1,0:T(8,128)}), f32[4,8,128]{2,1,0:T(8,128)}, u32[]{:S(2)}, u32[]{:S(2)}) async-start(f32[4,8,128]{2,1,0:T(8,128)} %concatenate.51), calls=%async_computation.1 | async-start | bytes 32768 | tf_op jit(solution)/shard_map/all_to_all | solution.py:21
  70.0 50.2 %copy-start.2 = (bf16[128,640]{1,0:T(8,128)(2,1)S(1)}, bf16[128,640]{1,0:T(8,128)(2,1)}, u32[]{:S(2)}) copy-start(bf16[128,640]{1,0:T(8,128)(2,1)} %param.32) | copy-start | bytes 491524
  70.0 50.4 %copy-start.3 = (bf16[128,640]{1,0:T(8,128)(2,1)S(1)}, bf16[128,640]{1,0:T(8,128)(2,1)}, u32[]{:S(2)}) copy-start(bf16[128,640]{1,0:T(8,128)(2,1)} %param.33) | copy-start | bytes 491524
  70.0 89.1 %copy-start.4 = (bf16[640,128]{1,0:T(8,128)(2,1)S(1)}, bf16[640,128]{1,0:T(8,128)(2,1)}, u32[]{:S(2)}) copy-start(bf16[640,128]{1,0:T(8,128)(2,1)} %param.34) | copy-start | bytes 491524
  93.6 9.4 %all-to-all-start.3 = ((bf16[4,256,128]{2,1,0:T(8,128)(2,1)}), bf16[4,256,128]{2,1,0:T(8,128)(2,1)S(1)}, u32[]{:S(2)}, u32[]{:S(2)}) async-start(bf16[4,256,128]{2,1,0:T(8,128)(2,1)} %broadcast_in_dim.103), calls=%async_computation.3 | async-start | bytes 524288 | tf_op jit(solution)/shard_map/all_to_all | solution.py:21
  104.5 15.5 %all-to-all-start.4 = ((bf16[64,8,128]{2,1,0:T(8,128)(2,1)}), bf16[64,8,128]{2,1,0:T(8,128)(2,1)S(1)}, u32[]{:S(2)}, u32[]{:S(2)}) async-start(bf16[64,8,128]{2,1,0:T(8,128)(2,1)} %bitcast.21), calls=%async_computation.4 | async-start | bytes 262144 | tf_op jit(solution)/shard_map/all_to_all | solution.py:21
